TPU v7x, 32 devices: a whole 2x2x4 slice. The times are simulated.
32 devices in a mesh: ep: 8 (over z, y), tp: 4 (over x, core).
Axes of the slice: x: 2, y: 2, z: 4, core: 2. Of those that a mesh axis runs over, the one named last changes fastest.
Arguments:
- tokens: bfloat16 [192, 2048], P('ep'), may hold values from -6 to 6
- delta_state: float32 [192, 8, 128, 128], P('ep', 'tp'), may hold values from -3 to 3
- first_gain: bfloat16 [2048], replicated, may hold values from 0.099609375 to 1.8984375
- query_weight: bfloat16 [2048, 1024], P(None, 'tp'), may hold values from -0.125 to 0.125
- key_weight: bfloat16 [2048, 1024], P(None, 'tp'), may hold values from -0.125 to 0.125
- value_weight: bfloat16 [2048, 1024], P(None, 'tp'), may hold values from -0.125 to 0.125
- outgate_weight: bfloat16 [2048, 1024], P(None, 'tp'), may hold values from -0.125 to 0.125
- beta_weight: bfloat16 [2048, 8], replicated, may hold values from -0.125 to 0.125
- decay_weight: bfloat16 [2048, 8], replicated, may hold values from -0.125 to 0.125
- decay_rate: float32 [8], replicated, may hold values from 0.05 to 4
- decay_bias: float32 [8], replicated, may hold values from -3 to 3
- head_gain: bfloat16 [128], replicated, may hold values from 0.099609375 to 1.8984375
- out_weight: bfloat16 [1024, 2048], P('tp'), may hold values from -0.1875 to 0.1875
- second_gain: bfloat16 [2048], replicated, may hold values from 0.099609375 to 1.8984375
- blend_weight: bfloat16 [2048], replicated, may hold values from -0.125 to 0.125
- dense_gate_weight: bfloat16 [2048, 2048], P(None, 'tp'), may hold values from -0.125 to 0.125
- dense_up_weight: bfloat16 [2048, 2048], P(None, 'tp'), may hold values from -0.125 to 0.125
- dense_down_weight: bfloat16 [2048, 2048], P('tp'), may hold values from -0.125 to 0.125
- expert_gate: bfloat16 [32, 2048, 512], P(('ep', 'tp')), may hold values from -0.125 to 0.125
- expert_up: bfloat16 [32, 2048, 512], P(('ep', 'tp')), may hold values from -0.125 to 0.125
- expert_down: bfloat16 [32, 512, 2048], P(('ep', 'tp')), may hold values from -0.25 to 0.25
- route_ids: int32 [192, 6], P('ep'), may hold values from 0 to 31, all different within a row; in each aligned block of 24 rows (0 to 23, 24 to 47, ...) at most 7 rows name the same one
- route_weights: float32 [192, 6], P('ep'), may hold values from 0.1 to 1
Outputs:
- new_tokens: bfloat16 [192, 2048], P('ep')
- new_state: float32 [192, 8, 128, 128], P('ep', 'tp')
Inputs may be any that keep to these rules, and one draw needn't show every extreme that they name: `route_ids`: each row names 6 different experts. In each aligned block of 24 rows (the sequences of one index of ep) no expert is named by more than 7 rows, and in some block an expert is named by exactly 7 rows.
All inputs are finite; a program needn't handle non-finite values.
Results may differ from a plain program's by a relative error of at most 0.017.
Values may be sent and summed in bfloat16 or wider, within the bound.
No kernel may reach another device: no remote copies, remote signals or barrier semaphores. Data moves between devices by JAX's collectives and lax.ppermute only.
A program may use at most 128 MiB of HBM per device.

v0:
```python
import jax
import jax.numpy as jnp
from jax import lax
from jax.sharding import PartitionSpec as P

norm_eps = 1e-06
unit_eps = 1e-06
routed_scale = 2.5


def rms_scale(values, gain):
    values = values.astype(jnp.float32)
    inverse = lax.rsqrt(jnp.mean(values * values, axis=-1, keepdims=True) + norm_eps)
    return values * inverse * gain.astype(jnp.float32)


def unit_rows(values):
    return values * lax.rsqrt(jnp.sum(values * values, axis=-1, keepdims=True) + unit_eps)


def rounded(values):
    return lax.optimization_barrier(values.astype(jnp.bfloat16)).astype(jnp.float32)


def delta_update(delta_state, query_raw, key_raw, value_raw, beta_gate, log_decay):
    head_size = delta_state.shape[-1]
    query_unit = unit_rows(jax.nn.silu(query_raw)) * head_size ** (-0.5)
    key_unit = unit_rows(jax.nn.silu(key_raw))
    value_act = jax.nn.silu(value_raw)
    decayed = jnp.exp(log_decay)[:, :, None, None] * delta_state
    predicted = jnp.einsum("shkv,shk->shv", decayed, key_unit, precision=lax.Precision.HIGHEST)
    update = (beta_gate[:, :, None] * key_unit)[:, :, :, None] * (value_act - predicted)[
        :, :, None, :
    ]
    new_state = decayed + update
    readout = jnp.einsum("shkv,shk->shv", new_state, query_unit, precision=lax.Precision.HIGHEST)
    return (new_state, readout)


def gated_heads(readout, outgate_raw, head_gain):
    scaled = rms_scale(readout, head_gain) * jax.nn.silu(outgate_raw)
    return scaled.reshape(scaled.shape[0], -1).astype(jnp.bfloat16)


def expert_rows(row_block, gate_mat, up_mat, down_mat):
    gate_part = jnp.dot(row_block, gate_mat, preferred_element_type=jnp.float32)
    up_part = jnp.dot(row_block, up_mat, preferred_element_type=jnp.float32)
    hidden = (jax.nn.silu(gate_part) * up_part).astype(jnp.bfloat16)
    return jnp.dot(hidden, down_mat, preferred_element_type=jnp.float32).astype(jnp.bfloat16)


def shards(
    tokens,
    delta_state,
    first_gain,
    query_weight,
    key_weight,
    value_weight,
    outgate_weight,
    beta_weight,
    decay_weight,
    decay_rate,
    decay_bias,
    head_gain,
    out_weight,
    second_gain,
    blend_weight,
    dense_gate_weight,
    dense_up_weight,
    dense_down_weight,
    expert_gate,
    expert_up,
    expert_down,
    route_ids,
    route_weights,
):
    seq_count = tokens.shape[0]
    head_local = delta_state.shape[1]
    head_size = delta_state.shape[2]
    top_count = route_ids.shape[1]
    ep_count = lax.axis_size("ep")
    tp_count = lax.axis_size("tp")
    tp_index = lax.axis_index("tp")
    normed = rms_scale(tokens, first_gain).astype(jnp.bfloat16)

    def project(weight):
        product = jnp.dot(normed, weight, preferred_element_type=jnp.float32)
        return rounded(product).reshape(seq_count, head_local, head_size)

    query_raw = project(query_weight)
    key_raw = project(key_weight)
    value_raw = project(value_weight)
    outgate_raw = project(outgate_weight)
    head_start = tp_index * head_local
    beta_all = jax.nn.sigmoid(jnp.dot(normed, beta_weight, preferred_element_type=jnp.float32))
    beta_gate = lax.dynamic_slice_in_dim(beta_all, head_start, head_local, 1)
    decay_input = jnp.dot(normed, decay_weight, preferred_element_type=jnp.float32) + decay_bias
    decay_all = -decay_rate * jax.nn.softplus(decay_input)
    log_decay = lax.dynamic_slice_in_dim(decay_all, head_start, head_local, 1)
    new_state, readout = delta_update(
        delta_state, query_raw, key_raw, value_raw, beta_gate, log_decay
    )
    gated = gated_heads(readout, outgate_raw, head_gain)
    mix_part = jnp.dot(gated, out_weight, preferred_element_type=jnp.float32)
    row_local = seq_count // tp_count
    mixed_rows = lax.psum_scatter(
        mix_part.astype(jnp.bfloat16), "tp", scatter_dimension=0, tiled=True
    ).astype(jnp.float32)
    own_tokens = lax.dynamic_slice_in_dim(tokens, tp_index * row_local, row_local, 0)
    residual_rows = (own_tokens.astype(jnp.float32) + mixed_rows).astype(jnp.bfloat16)
    normed_rows = rms_scale(residual_rows, second_gain).astype(jnp.bfloat16)
    normed_mid, residual = (
        lax.all_gather(normed_rows, "tp", axis=0, tiled=True),
        lax.all_gather(residual_rows, "tp", axis=0, tiled=True),
    )
    blend_gate = jax.nn.sigmoid(
        jnp.dot(normed_mid, blend_weight, preferred_element_type=jnp.float32)
    )
    dense_gate_raw = jnp.dot(normed_mid, dense_gate_weight, preferred_element_type=jnp.float32)
    dense_up_raw = jnp.dot(normed_mid, dense_up_weight, preferred_element_type=jnp.float32)
    dense_hidden = (jax.nn.silu(dense_gate_raw) * dense_up_raw).astype(jnp.bfloat16)
    dense_part = jnp.dot(dense_hidden, dense_down_weight, preferred_element_type=jnp.float32)
    expert_count = ep_count * tp_count
    capacity = max(2, (3 * seq_count * top_count + 2 * expert_count - 1) // (2 * expert_count))
    flat_ids = route_ids.reshape(-1)
    assign_count = flat_ids.shape[0]
    earlier = jnp.arange(assign_count)[:, None] > jnp.arange(assign_count)[None, :]
    matches = (flat_ids[:, None] == flat_ids[None, :]) & earlier
    rank_of = jnp.sum(matches.astype(jnp.int32), axis=1)
    owned = flat_ids % tp_count == tp_index
    slot_of = jnp.where(owned, flat_ids // tp_count * capacity + rank_of, -1)
    slot_total = ep_count * capacity
    slot_grid = slot_of.reshape(seq_count, top_count)
    slot_range = jnp.arange(slot_total, dtype=jnp.int32)
    dispatch = jnp.any(slot_grid[None, :, :] == slot_range[:, None, None], axis=2).astype(
        jnp.bfloat16
    )
    model_width = normed_mid.shape[1]
    outgoing = jnp.dot(dispatch, normed_mid, preferred_element_type=jnp.float32).astype(
        jnp.bfloat16
    )
    outgoing = outgoing.reshape(ep_count, capacity, model_width)
    arrived = lax.all_to_all(outgoing, "ep", split_axis=0, concat_axis=0, tiled=True)
    result = expert_rows(
        arrived.reshape(-1, model_width), expert_gate[0], expert_up[0], expert_down[0]
    )
    returned = lax.all_to_all(
        result.reshape(arrived.shape), "ep", split_axis=0, concat_axis=0, tiled=True
    )
    returned_rows = returned.reshape(slot_total, model_width)
    picked = returned_rows[jnp.maximum(slot_of, 0)].astype(jnp.float32)
    picked = picked.reshape(seq_count, top_count, model_width)
    route_scale = route_weights / jnp.sum(route_weights, axis=1, keepdims=True) * routed_scale
    kept_scale = jnp.where(owned.reshape(seq_count, top_count), route_scale, 0.0)
    routed_part = jnp.sum(kept_scale[:, :, None] * picked, axis=1)
    combined = lax.psum(
        (routed_part + blend_gate[:, None] * dense_part).astype(jnp.bfloat16), "tp"
    ).astype(jnp.float32)
    new_tokens = (residual.astype(jnp.float32) + combined).astype(jnp.bfloat16)
    return (new_tokens, new_state)


def solution(mesh):
    placed = (
        P("ep", None),
        P("ep", "tp", None, None),
        P(),
        P(None, "tp"),
        P(None, "tp"),
        P(None, "tp"),
        P(None, "tp"),
        P(),
        P(),
        P(),
        P(),
        P(),
        P("tp", None),
        P(),
        P(),
        P(None, "tp"),
        P(None, "tp"),
        P("tp", None),
        P(("ep", "tp"), None, None),
        P(("ep", "tp"), None, None),
        P(("ep", "tp"), None, None),
        P("ep", None),
        P("ep", None),
    )
    return jax.shard_map(
        shards,
        mesh=mesh,
        in_specs=placed,
        out_specs=(P("ep", None), P("ep", "tp", None, None)),
        check_vma=False,
    )
```

profile of v0, /device:TPU:0, one launch (start us, length us, event | category | flops | bytes accessed | tf_op | source)
XLA Modules:
  0.0 129.9 jit_solution(16252030878266203387)
XLA Ops:
  7.2 0.0 copy-start
  7.2 0.0 copy-start.3
  7.2 0.8 convert_element_type.92
  8.0 1.1 fusion.27
  9.1 0.7 neg.38
  9.8 1.1 fusion.22
  10.9 1.2 fusion.59
  12.1 0.1 copy.48
  12.2 1.6 %convolution_convert_fusion.6 = bf16[24,256]{1,0:T(8,128)(2,1)S(1)} fusion(bf16[2048,256]{1,0:T(8,128)(2,1)} %param.27, bf16[24,2048]{1,0:T(8,128)(2,1)} %param.23, f32[2048]{0:T(1024)S(1)} %convert_element_type.92, f32[24]{0:T(128)S(1)} %add_rsqrt_fusion.4), kind=kOutput, calls=%fused_computation.24 | convolution fusion | flops 25368576 | bytes 1167456 | tf_op jit(solution)/shard_map/dot_general | solution.py:87
  13.8 0.1 multiply_reduce_fusion.3
  13.9 0.1 copy.47
  14.0 1.6 %convolution_convert_fusion.5 = bf16[24,256]{1,0:T(8,128)(2,1)S(1)} fusion(bf16[2048,256]{1,0:T(8,128)(2,1)} %param.28, bf16[24,2048]{1,0:T(8,128)(2,1)} %param.23, f32[2048]{0:T(1024)S(1)} %convert_element_type.92, f32[24]{0:T(128)S(1)} %add_rsqrt_fusion.4), kind=kOutput, calls=%fused_computation.23 | convolution fusion | flops 25368576 | bytes 1167456 | tf_op jit(solution)/shard_map/dot_general | solution.py:87
  15.6 0.3 convolution_convert_fusion.4
  16.0 0.1 multiply_reduce_fusion.2
  16.1 0.1 broadcast_multiply_fusion.1
  16.2 4.9 %fusion.1 = f32[24,2,1,128]{3,2,1,0:T(1,128)S(1)} fusion(f32[24,2,128,1]{2,3,1,0:T(1,128)S(1)} %bitcast.71, f32[24,2,128,128]{3,2,1,0:T(8,128)} %param.24, f32[24,2]{1,0:T(8,128)S(1)} %copy.47), kind=kOutput, calls=%fused_computation.2 | convolution fusion | flops 10223616 | bytes 3195072 | tf_op jit(solution)/shard_map/shkv,shk->shv/dot_general | solution.py:31
  21.2 1.1 multiply_add_fusion
  22.3 0.0 copy-start.2
  22.4 0.1 multiply_multiply_fusion
  22.5 1.5 %copy-done.2 = f32[24,2,128,128]{3,2,1,0:T(8,128)} copy-done((f32[24,2,128,128]{3,2,1,0:T(8,128)}, f32[24,2,128,128]{3,2,1,0:T(8,128)S(1)}, u32[]{:S(2)}) %copy-start.2) | copy-done | bytes 3145752
  24.0 2.8 %fusion.69 = f32[24,2,1,128]{3,2,1,0:T(1,128)S(1)} fusion(f32[24,2,128,128]{3,2,1,0:T(8,128)S(1)} %multiply_add_fusion, f32[24,2,128,1]{2,3,1,0:T(1,128)S(1)} %bitcast.73), kind=kOutput, calls=%fused_computation.112 | convolution fusion | flops 9437184 | bytes 3194880 | tf_op jit(solution)/shard_map/shkv,shk->shv/dot_general | solution.py:36
  26.8 0.1 multiply_reduce_fusion.1
  26.9 0.3 convolution_convert_fusion.3
  27.2 0.0 copy-start.9
  27.3 0.1 fusion.50
  27.4 0.2 convolution_convert_fusion.2
  27.6 9.7 %fusion = bf16[8,2048]{1,0:T(8,128)(2,1)S(1)} fusion(bf16[24,2048]{1,0:T(8,128)(2,1)S(1)} %convolution_convert_fusion.2), kind=kCustom, calls=%all-reduce-scatter | all-reduce-scatter fusion | flops 65537 | bytes 131584
  37.3 1.3 collective-permute-start
  38.6 0.1 copy.49
  38.7 0.1 eq.52
  38.8 0.2 convert_reduce_fusion
  39.0 0.1 reduce_sum.82
  39.1 0.1 copy.55
  39.2 0.1 fusion.36
  39.3 0.1 reshape.273
  39.5 0.6 dynamic-slice.4
  40.7 0.2 concatenate
  40.9 0.2 fusion.37
  41.0 0.1 fusion.46
  41.1 7.0 %all-gather.1 = bf16[4,6,2048]{2,1,0:T(8,128)(2,1)S(1)} all-gather(bf16[1,6,2048]{2,1,0:T(8,128)(2,1)S(1)} %fusion.46), channel_id=1, replica_groups=mesh['ep'=8,'tp'=4] {'tp'}, dimensions={0}, use_global_device_ids=true | all-gather | bytes 122880 | tf_op jit(solution)/shard_map/all_gather | solution.py:113
  48.1 0.3 convolution_convert_fusion.1
  48.4 0.8 reshape.269
  49.2 5.8 %all-to-all-start = ((bf16[8,7,2048]{2,1,0:T(8,128)(2,1)}), bf16[8,7,2048]{2,1,0:T(8,128)(2,1)S(1)}, u32[]{:S(2)}, u32[]{:S(2)}) async-start(bf16[8,7,2048]{2,1,0:T(8,128)(2,1)} %reshape.269), calls=%async_computation | async-start | bytes 524288 | tf_op jit(solution)/shard_map/all_to_all | solution.py:143
  55.0 0.1 copy.52
  55.2 0.1 multiply_select_fusion
  55.2 9.2 %all-to-all-done = bf16[8,7,2048]{2,1,0:T(8,128)(2,1)S(1)} async-done(((bf16[8,7,2048]{2,1,0:T(8,128)(2,1)}), bf16[8,7,2048]{2,1,0:T(8,128)(2,1)S(1)}, u32[]{:S(2)}, u32[]{:S(2)}) %all-to-all-start) | async-done | bytes 229408 | tf_op jit(solution)/shard_map/all_to_all | solution.py:143
  64.4 0.1 reshape.270
  64.5 2.0 %fusion.8 = f32[56,512]{1,0:T(8,128)S(1)} fusion(bf16[56,2048]{1,0:T(8,128)(2,1)S(1)} %reshape.270, bf16[1,2048,512]{2,1,0:T(8,128)(2,1)} %param.41), kind=kOutput, calls=%fused_computation.13 | convolution fusion | flops 117440512 | bytes 2441216 | tf_op jit(solution)/shard_map/dot_general | solution.py:46
  66.6 2.5 %convolution_convert_fusion = bf16[56,2048]{1,0:T(8,128)(2,1)S(1)} fusion(bf16[1,512,2048]{2,1,0:T(8,128)(2,1)S(1)} %copy-done, bf16[56,2048]{1,0:T(8,128)(2,1)S(1)} %reshape.270, bf16[1,2048,512]{2,1,0:T(8,128)(2,1)} %param.42, f32[56,512]{1,0:T(8,128)S(1)} %fusion.8), kind=kOutput, calls=%fused_computation.4 | convolution fusion | flops 235167744 | bytes 4767744 | tf_op jit(solution)/shard_map/dot_general | solution.py:49
  69.1 0.8 reshape.271
  69.8 3.6 %all-to-all-start.1 = ((bf16[8,7,2048]{2,1,0:T(8,128)(2,1)}), bf16[8,7,2048]{2,1,0:T(8,128)(2,1)S(1)}, u32[]{:S(2)}, u32[]{:S(2)}) async-start(bf16[8,7,2048]{2,1,0:T(8,128)(2,1)} %reshape.271), calls=%async_computation.1 | async-start | bytes 524288 | tf_op jit(solution)/shard_map/all_to_all | solution.py:147
  73.4 0.2 all-reduce.4.cloned.1.call-start
  73.6 0.1 fusion.26
  73.8 2.0 %fusion.70 = f32[24,512]{1,0:T(8,128)S(1)} fusion(bf16[24,2048]{1,0:T(8,128)(2,1)S(1)} %reshape.294, bf16[2048,512]{1,0:T(8,128)(2,1)} %param.38), kind=kOutput, calls=%fused_computation.113 | convolution fusion | flops 50331648 | bytes 2244608 | tf_op jit(solution)/shard_map/dot_general | solution.py:119
  75.8 6.6 %all-to-all-done.1 = bf16[8,7,2048]{2,1,0:T(8,128)(2,1)S(1)} async-done(((bf16[8,7,2048]{2,1,0:T(8,128)(2,1)}), bf16[8,7,2048]{2,1,0:T(8,128)(2,1)S(1)}, u32[]{:S(2)}, u32[]{:S(2)}) %all-to-all-start.1) | async-done | bytes 229408 | tf_op jit(solution)/shard_map/all_to_all | solution.py:147
  82.4 0.1 reshape.272
  82.5 1.0 gather_fusion
  83.5 1.3 %reshape.282 = f32[24,6,2048]{2,1,0:T(8,128)} reshape(bf16[144,2048]{1,0:T(8,128)(2,1)S(1)} %gather_fusion) | data formatting | bytes 1769472 | tf_op jit(solution)/shard_map/convert_element_type | solution.py:151
  84.8 2.0 %multiply_reduce_fusion = f32[24,2048]{1,0:T(8,128)S(1)} fusion(f32[24,6,2048]{2,1,0:T(8,128)} %reshape.282, f32[24,6]{1,0:T(8,128)S(1)} %multiply_select_fusion), kind=kLoop, calls=%fused_computation.15 | loop fusion | flops 540672 | bytes 1376832 | tf_op jit(solution)/shard_map/reduce_sum | solution.py:155
  86.8 3.6 %fusion.4 = bf16[24,2048]{1,0:T(8,128)(2,1)} fusion(f32[24,2048]{1,0:T(8,128)S(1)} %multiply_reduce_fusion, bf16[512,2048]{1,0:T(8,128)(2,1)} %param.40, bf16[24,2048]{1,0:T(8,128)(2,1)S(1)} %reshape.294, bf16[2048,512]{1,0:T(8,128)(2,1)} %param.39, f32[24]{0:T(128)S(1)} %fusion.26, f32[24,512]{1,0:T(8,128)S(1)} %fusion.70), kind=kOutput, calls=%fused_computation.8 | convolution fusion | flops 100884480 | bytes 4636768 | tf_op jit(solution)/shard_map/dot_general | solution.py:122
  90.4 0.0 all-reduce.4.cloned.1.call-update
  90.4 5.4 %all-gather = bf16[4,6,2048]{2,1,0:T(8,128)(2,1)S(1)} all-gather(bf16[1,6,2048]{2,1,0:T(8,128)(2,1)S(1)} %bitcast.68), channel_id=1, replica_groups=mesh['ep'=8,'tp'=4] {'tp'}, dimensions={0}, use_global_device_ids=true | all-gather | bytes 122880 | tf_op jit(solution)/shard_map/all_gather | solution.py:114
  95.9 25.7 %all-reduce.4.cloned.1.call-done = bf16[24,2048]{1,0:T(8,128)(2,1)} async-done(((bf16[24,2048]{1,0:T(8,128)(2,1)}), bf16[24,2048]{1,0:T(8,128)(2,1)}) %all-reduce.4.cloned.1.call-update) | async-done | bytes 98320 | tf_op jit(solution)/shard_map/psum | solution.py:156
  121.5 1.6 %add_convert_fusion = bf16[24,2048]{1,0:T(8,128)(2,1)} fusion(f32[24,2048]{1,0:T(8,128)S(1)} %reshape.295, bf16[24,2048]{1,0:T(8,128)(2,1)} %all-reduce.4.cloned.1.call-done), kind=kLoop, calls=%fused_computation.40 | loop fusion | flops 147456 | bytes 393216 | tf_op jit(solution)/shard_map/convert_element_type | solution.py:159
  (43 shorter events, 0.4 us)
Async XLA Ops:
  7.2 59.4 %copy-start = (bf16[1,512,2048]{2,1,0:T(8,128)(2,1)S(1)}, bf16[1,512,2048]{2,1,0:T(8,128)(2,1)}, u32[]{:S(2)}) copy-start(bf16[1,512,2048]{2,1,0:T(8,128)(2,1)} %param.43) | copy-start | bytes 6291460
  7.2 8.4 %copy-start.3 = (bf16[24,2048]{1,0:T(8,128)(2,1)S(1)}, bf16[24,2048]{1,0:T(8,128)(2,1)}, u32[]{:S(2)}) copy-start(bf16[24,2048]{1,0:T(8,128)(2,1)} %param.23) | copy-start | bytes 294916
  7.2 8.4 %copy-start.4 = (bf16[2048,256]{1,0:T(8,128)(2,1)S(1)}, bf16[2048,256]{1,0:T(8,128)(2,1)}, u32[]{:S(2)}) copy-start(bf16[2048,256]{1,0:T(8,128)(2,1)} %param.26) | copy-start | bytes 3145732
  16.0 5.3 %copy-start.1 = (f32[24,2,128,128]{3,2,1,0:T(8,128)S(1)}, f32[24,2,128,128]{3,2,1,0:T(8,128)}, u32[]{:S(2)}) copy-start(f32[24,2,128,128]{3,2,1,0:T(8,128)} %param.24) | copy-start | bytes 9437188
  22.3 1.7 %copy-start.2 = (f32[24,2,128,128]{3,2,1,0:T(8,128)}, f32[24,2,128,128]{3,2,1,0:T(8,128)S(1)}, u32[]{:S(2)}) copy-start(f32[24,2,128,128]{3,2,1,0:T(8,128)S(1)} %multiply_add_fusion) | copy-start | bytes 9437188
  22.4 4.6 %copy-start.5 = (bf16[2048,256]{1,0:T(8,128)(2,1)S(1)}, bf16[2048,256]{1,0:T(8,128)(2,1)}, u32[]{:S(2)}) copy-start(bf16[2048,256]{1,0:T(8,128)(2,1)} %param.29) | copy-start | bytes 3145732
  24.0 3.3 %copy-start.12 = (bf16[128]{0:T(256)(128)(2,1)S(1)}, bf16[128]{0:T(256)(128)(2,1)}, u32[]{:S(2)}) copy-start(bf16[128]{0:T(256)(128)(2,1)} %param.34) | copy-start | bytes 772
  24.0 3.4 %copy-start.6 = (bf16[256,2048]{1,0:T(8,128)(2,1)S(1)}, bf16[256,2048]{1,0:T(8,128)(2,1)}, u32[]{:S(2)}) copy-start(bf16[256,2048]{1,0:T(8,128)(2,1)} %param.35) | copy-start | bytes 3145732
  26.8 11.8 %copy-start.10 = (s32[24,6]{0,1:T(8,128)S(1)}, s32[24,6]{0,1:T(8,128)}, u32[]{:S(2)}) copy-start(s32[24,6]{0,1:T(8,128)} %param.44) | copy-start | bytes 1732
  26.8 12.6 %copy-start.8 = (bf16[2048]{0:T(1024)(128)(2,1)S(1)}, bf16[2048]{0:T(1024)(128)(2,1)}, u32[]{:S(2)}) copy-start(bf16[2048]{0:T(1024)(128)(2,1)} %param.36) | copy-start | bytes 12292
  26.8 12.7 %copy-start.11 = (u32[32]{0:T(128)S(1)}, u32[32]{0:T(128)}, u32[]{:S(2)}) copy-start(u32[32]{0:T(128)} %constant.90) | copy-start | bytes 388
  27.2 27.8 %copy-start.7 = (f32[24,6]{0,1:T(8,128)S(1)}, f32[24,6]{0,1:T(8,128)}, u32[]{:S(2)}) copy-start(f32[24,6]{0,1:T(8,128)} %param.45) | copy-start | bytes 1732
  27.2 27.9 %copy-start.9 = (bf16[2048]{0:T(1024)(128)(2,1)S(1)}, bf16[2048]{0:T(1024)(128)(2,1)}, u32[]{:S(2)}) copy-start(bf16[2048]{0:T(1024)(128)(2,1)} %param.37) | copy-start | bytes 12292
  37.3 3.4 %collective-permute-start = (bf16[6,2048]{1,0:T(8,128)(2,1)S(1)}, bf16[6,2048]{1,0:T(8,128)(2,1)S(1)}, u32[]{:S(2)}, u32[]{:S(2)}) collective-permute-start(bf16[6,2048]{1,0:T(8,128)(2,1)S(1)} %slice.2), channel_id=1, source_target_pairs={{0,1},{1,2},{2,3},{4,5},{5,6},{6,7},{8,9},{9,10},{10,11},{12,13},{... | collective-permute-start | bytes 73736
  49.2 15.3 %all-to-all-start = ((bf16[8,7,2048]{2,1,0:T(8,128)(2,1)}), bf16[8,7,2048]{2,1,0:T(8,128)(2,1)S(1)}, u32[]{:S(2)}, u32[]{:S(2)}) async-start(bf16[8,7,2048]{2,1,0:T(8,128)(2,1)} %reshape.269), calls=%async_computation | async-start | bytes 524288 | tf_op jit(solution)/shard_map/all_to_all | solution.py:143
  69.8 12.6 %all-to-all-start.1 = ((bf16[8,7,2048]{2,1,0:T(8,128)(2,1)}), bf16[8,7,2048]{2,1,0:T(8,128)(2,1)S(1)}, u32[]{:S(2)}, u32[]{:S(2)}) async-start(bf16[8,7,2048]{2,1,0:T(8,128)(2,1)} %reshape.271), calls=%async_computation.1 | async-start | bytes 524288 | tf_op jit(solution)/shard_map/all_to_all | solution.py:147
  73.4 48.1 %all-reduce.4.cloned.1.call-start = ((), (), s32[]{:S(2)}) async-start(), calls=%async_computation.2 | async-start | bytes 196608 | tf_op jit(solution)/shard_map/psum | solution.py:156
Sparse Core Ops, SparseCore 0:
  90.5 30.9 all-reduce.3
where the time goes:
time: 131 us; the launch traced here: 130 us
  waiting for transfers between devices  41.5 us (32%)
  matrix products  24.5 us (19%)
  blocking collectives  22 us (17%)
  between operations  15.1 us (12%)
  starting transfers between devices  10.9 us (8%)
  other arithmetic  8.59 us (7%)
  local copies, waits for them, and re-layouts  7.27 us (6%)
    psum x1, waiting for transfers between devices, shards(): lax.psum((routed_part + blend_gate[:, None] * dense_part).astype(jnp.bflo...  25.7 us
    unnamed x1, blocking collectives  9.66 us
    all_to_all x1, waiting for transfers between devices, shards(): lax.all_to_all(outgoing, 'ep', split_axis=0, concat_axis=0, tiled=True)  9.18 us
    all_gather x1, blocking collectives, shards(): lax.all_gather(normed_rows, 'tp', axis=0, tiled=True)  6.97 us
    all_to_all x1, waiting for transfers between devices, shards(): lax.all_to_all(result.reshape(arrived.shape), 'ep', split_axis=0, concat_...  6.63 us
    all_to_all x1, starting transfers between devices, shards(): lax.all_to_all(outgoing, 'ep', split_axis=0, concat_axis=0, tiled=True)  5.83 us
    all_gather x1, blocking collectives, shards(): lax.all_gather(residual_rows, 'tp', axis=0, tiled=True)  5.42 us
    dot_general x1, matrix products, delta_update(): jnp.einsum('shkv,shk->shv', decayed, key_unit, precision=lax.Precision.HI...  4.94 us
  transfers between devices with their start and end apart: 4, of which 3 were waited for; matrix products, arithmetic and copies ran while one was open for 3% of the time, Pallas kernels for 0%

commit v1 on v0

--- a/solution.py
+++ b/solution.py
@@ -40,6 +40,11 @@
 def gated_heads(readout, outgate_raw, head_gain):
     scaled = rms_scale(readout, head_gain) * jax.nn.silu(outgate_raw)
     return scaled.reshape(scaled.shape[0], -1).astype(jnp.bfloat16)
+
+
+def tp_sum(part):
+    parts = lax.all_gather(part.astype(jnp.bfloat16), "tp", axis=0, tiled=False)
+    return jnp.sum(parts.astype(jnp.float32), axis=0)
 
 
 def expert_rows(row_block, gate_mat, up_mat, down_mat):
@@ -102,17 +107,8 @@
     )
     gated = gated_heads(readout, outgate_raw, head_gain)
     mix_part = jnp.dot(gated, out_weight, preferred_element_type=jnp.float32)
-    row_local = seq_count // tp_count
-    mixed_rows = lax.psum_scatter(
-        mix_part.astype(jnp.bfloat16), "tp", scatter_dimension=0, tiled=True
-    ).astype(jnp.float32)
-    own_tokens = lax.dynamic_slice_in_dim(tokens, tp_index * row_local, row_local, 0)
-    residual_rows = (own_tokens.astype(jnp.float32) + mixed_rows).astype(jnp.bfloat16)
-    normed_rows = rms_scale(residual_rows, second_gain).astype(jnp.bfloat16)
-    normed_mid, residual = (
-        lax.all_gather(normed_rows, "tp", axis=0, tiled=True),
-        lax.all_gather(residual_rows, "tp", axis=0, tiled=True),
-    )
+    residual = (tokens.astype(jnp.float32) + tp_sum(mix_part)).astype(jnp.bfloat16)
+    normed_mid = rms_scale(residual, second_gain).astype(jnp.bfloat16)
     blend_gate = jax.nn.sigmoid(
         jnp.dot(normed_mid, blend_weight, preferred_element_type=jnp.float32)
     )
@@ -148,14 +144,19 @@
         result.reshape(arrived.shape), "ep", split_axis=0, concat_axis=0, tiled=True
     )
     returned_rows = returned.reshape(slot_total, model_width)
-    picked = returned_rows[jnp.maximum(slot_of, 0)].astype(jnp.float32)
-    picked = picked.reshape(seq_count, top_count, model_width)
     route_scale = route_weights / jnp.sum(route_weights, axis=1, keepdims=True) * routed_scale
-    kept_scale = jnp.where(owned.reshape(seq_count, top_count), route_scale, 0.0)
-    routed_part = jnp.sum(kept_scale[:, :, None] * picked, axis=1)
-    combined = lax.psum(
-        (routed_part + blend_gate[:, None] * dense_part).astype(jnp.bfloat16), "tp"
-    ).astype(jnp.float32)
+    spread = jnp.sum(
+        jnp.where(slot_grid[:, :, None] == slot_range, route_scale[:, :, None], 0.0), axis=1
+    )
+    spread_high = lax.reduce_precision(spread, 8, 7)
+    routed_part = jnp.dot(
+        spread_high.astype(jnp.bfloat16), returned_rows, preferred_element_type=jnp.float32
+    ) + jnp.dot(
+        (spread - spread_high).astype(jnp.bfloat16),
+        returned_rows,
+        preferred_element_type=jnp.float32,
+    )
+    combined = tp_sum(routed_part + blend_gate[:, None] * dense_part)
     new_tokens = (residual.astype(jnp.float32) + combined).astype(jnp.bfloat16)
     return (new_tokens, new_state)
 

time: 131 us -> 72.2 us (0.55)
  waiting for transfers between devices: 41.5 us -> 13 us
  between operations: 15.1 us -> 1.01 us
  blocking collectives: 22 us -> 14.1 us
  local copies, waits for them, and re-layouts: 7.27 us -> 3.98 us
  other arithmetic: 8.59 us -> 5.76 us
  starting transfers between devices: 10.9 us -> 9.42 us
    psum x1 -> x0, waiting for transfers between devices: 25.7 us -> none  [shards(): lax.psum((routed_part + blend_gate[:, None] * dense_part).astype(jnp.bflo...]
    unnamed x1 -> x0, blocking collectives: 9.66 us -> none
    all_to_all x1, waiting for transfers between devices: 9.18 us -> 7.12 us  [shards(): lax.all_to_all(outgoing, 'ep', split_axis=0, concat_axis=0, tiled=True)]
    reduce_sum x1 -> x3, other arithmetic: 1.97 us -> 0.2 us  [the longest x1 0.1 us: shards(): jnp.sum(jnp.where(slot_grid[:, :, None] == slot_range, route_scale[:, :,...]
    all_gather x2, blocking collectives: 12.4 us -> 14.1 us  [tp_sum(): parts = lax.all_gather(part.astype(jnp.bfloat16), 'tp', axis=0, tiled=False)]
    convert_element_type x2 -> x0, local copies, waits for them, and re-layouts: 1.33 us -> none  [the longest x1 1.3 us: shards(): picked = returned_rows[jnp.maximum(slot_of, 0)].astype(jnp.float32)]
  transfers between devices with their start and end apart: 4 -> 2, of which waited for: 3 -> 2; matrix products, arithmetic and copies ran while one was open for 3% -> 8% of each run, Pallas kernels for 0% -> 0%
where the time goes in v1:
time: 72.2 us; the launch traced here: 71.6 us
  matrix products  24.4 us (34%)
  blocking collectives  14.1 us (20%)
  waiting for transfers between devices  13 us (18%)
  starting transfers between devices  9.42 us (13%)
  other arithmetic  5.76 us (8%)
  local copies, waits for them, and re-layouts  3.98 us (6%)
  between operations  1.01 us (1%)
    all_gather x2, blocking collectives, tp_sum(): parts = lax.all_gather(part.astype(jnp.bfloat16), 'tp', axis=0, tiled=False)  14.1 us
    all_to_all x1, waiting for transfers between devices, shards(): lax.all_to_all(outgoing, 'ep', split_axis=0, concat_axis=0, tiled=True)  7.12 us
    all_to_all x1, waiting for transfers between devices, shards(): lax.all_to_all(result.reshape(arrived.shape), 'ep', split_axis=0, concat_...  5.87 us
    all_to_all x1, starting transfers between devices, shards(): lax.all_to_all(outgoing, 'ep', split_axis=0, concat_axis=0, tiled=True)  5.83 us
    dot_general x1, matrix products, delta_update(): jnp.einsum('shkv,shk->shv', decayed, key_unit, precision=lax.Precision.HI...  4.94 us
    dot_general x4, matrix products, project(): product = jnp.dot(normed, weight, preferred_element_type=jnp.float32)  3.74 us
    all_to_all x1, starting transfers between devices, shards(): lax.all_to_all(result.reshape(arrived.shape), 'ep', split_axis=0, concat_...  3.59 us
    dot_general x1, matrix products, shards(): jnp.dot(dense_hidden, dense_down_weight, preferred_element_type=jnp.float32)  3.01 us
  transfers between devices with their start and end apart: 2, of which 2 were waited for; matrix products, arithmetic and copies ran while one was open for 8% of the time, Pallas kernels for 0%

profile of v1, /device:TPU:0, one launch (start us, length us, event | category | flops | bytes accessed | tf_op | source)
XLA Modules:
  0.0 71.6 jit_solution(9187327230261243915)
XLA Ops:
  0.6 0.0 copy-start
  0.6 0.0 copy-start.3
  0.7 0.0 copy-start.4
  0.7 0.8 %convert_element_type.86 = f32[2048]{0:T(1024)S(1)} convert(bf16[2048]{0:T(1024)(128)(2,1)} %param.25) | non-fusion elementwise | flops 2048 | bytes 12288 | tf_op jit(solution)/shard_map/convert_element_type | solution.py:14
  1.5 1.1 %fusion.26 = f32[24]{0:T(128)S(1)} fusion(bf16[24,2048]{1,0:T(8,128)(2,1)} %param.23), kind=kLoop, calls=%fused_computation.42 | loop fusion | flops 147432 | bytes 98400 | tf_op jit(solution)/shard_map/reduce_sum | solution.py:13
  2.6 0.7 neg.38
  3.3 1.1 %fusion.21 = f32[24,8]{0,1:T(8,128)S(1)} fusion(bf16[2048,8]{0,1:T(8,128)(2,1)} %param.30, bf16[24,2048]{1,0:T(8,128)(2,1)} %param.23, f32[2048]{0:T(1024)S(1)} %convert_element_type.86, f32[24]{0:T(128)S(1)} %add_rsqrt_fusion.4), kind=kOutput, calls=%fused_computation.27 | convolution fusion | flops 983616 | bytes 140128 | tf_op jit(solution)/shard_map/dot_general | solution.py:100
  4.4 1.2 %fusion.62 = f32[24,8]{0,1:T(8,128)S(1)} fusion(bf16[2048,8]{0,1:T(8,128)(2,1)} %param.31, f32[8]{0:T(128)} %param.33, f32[8]{0:T(128)S(1)} %neg.38, bf16[24,2048]{1,0:T(8,128)(2,1)} %param.23, f32[2048]{0:T(1024)S(1)} %convert_element_type.86, f32[24]{0:T(128)S(1)} %add_rsqrt_fusion.4), kind=kOutput, calls=%fused_computation.104 | convolution fusion | flops 984576 | bytes 140192 | tf_op jit(solution)/shard_map/dot_general | solution.py:102
  5.6 0.1 copy.39
  5.6 1.6 %convolution_convert_fusion.6 = bf16[24,256]{1,0:T(8,128)(2,1)S(1)} fusion(bf16[2048,256]{1,0:T(8,128)(2,1)} %param.27, bf16[24,2048]{1,0:T(8,128)(2,1)} %param.23, f32[2048]{0:T(1024)S(1)} %convert_element_type.86, f32[24]{0:T(128)S(1)} %add_rsqrt_fusion.4), kind=kOutput, calls=%fused_computation.23 | convolution fusion | flops 25368576 | bytes 1167456 | tf_op jit(solution)/shard_map/dot_general | solution.py:92
  7.3 0.1 multiply_reduce_fusion.2
  7.4 0.1 copy.38
  7.5 1.6 %convolution_convert_fusion.5 = bf16[24,256]{1,0:T(8,128)(2,1)S(1)} fusion(bf16[2048,256]{1,0:T(8,128)(2,1)} %param.28, bf16[24,2048]{1,0:T(8,128)(2,1)} %param.23, f32[2048]{0:T(1024)S(1)} %convert_element_type.86, f32[24]{0:T(128)S(1)} %add_rsqrt_fusion.4), kind=kOutput, calls=%fused_computation.22 | convolution fusion | flops 25368576 | bytes 1167456 | tf_op jit(solution)/shard_map/dot_general | solution.py:92
  9.1 0.0 copy-done.3
  9.1 0.0 copy-done.4
  9.1 0.3 convolution_convert_fusion.4
  9.4 0.0 copy-start.1
  9.4 0.1 multiply_reduce_fusion.1
  9.6 0.1 broadcast_multiply_fusion.1
  9.7 4.9 %fusion = f32[24,2,1,128]{3,2,1,0:T(1,128)S(1)} fusion(f32[24,2,128,1]{2,3,1,0:T(1,128)S(1)} %bitcast.66, f32[24,2,128,128]{3,2,1,0:T(8,128)} %param.24, f32[24,2]{1,0:T(8,128)S(1)} %copy.38), kind=kOutput, calls=%fused_computation.1 | convolution fusion | flops 10223616 | bytes 3195072 | tf_op jit(solution)/shard_map/shkv,shk->shv/dot_general | solution.py:31
  14.7 0.0 copy-done.1
  14.7 1.1 %multiply_add_fusion = f32[24,2,128,128]{3,2,1,0:T(8,128)S(1)} fusion(f32[24,2,128,128]{3,2,1,0:T(8,128)S(1)} %copy-done.1, f32[24,2,128]{2,1,0:T(2,128)S(1)} %fusion.47, f32[24,2,128]{2,1,0:T(2,128)S(1)} %get-tuple-element.6, f32[24,2]{1,0:T(8,128)S(1)} %copy.38), kind=kLoop, calls=%fused_computation | loop fusion | flops 2359296 | bytes 6340800 | tf_op jit(solution)/shard_map/add | solution.py:35
  15.8 0.0 copy-start.2
  15.8 0.0 copy-start.5
  15.8 0.1 multiply_multiply_fusion
  15.9 1.5 %copy-done.2 = f32[24,2,128,128]{3,2,1,0:T(8,128)} copy-done((f32[24,2,128,128]{3,2,1,0:T(8,128)}, f32[24,2,128,128]{3,2,1,0:T(8,128)S(1)}, u32[]{:S(2)}) %copy-start.2) | copy-done | bytes 3145752
  17.5 2.8 %fusion.78 = f32[24,2,1,128]{3,2,1,0:T(1,128)S(1)} fusion(f32[24,2,128,128]{3,2,1,0:T(8,128)S(1)} %multiply_add_fusion, f32[24,2,128,1]{2,3,1,0:T(1,128)S(1)} %bitcast.68), kind=kOutput, calls=%fused_computation.113 | convolution fusion | flops 9437184 | bytes 3194880 | tf_op jit(solution)/shard_map/shkv,shk->shv/dot_general | solution.py:36
  20.3 0.1 multiply_reduce_fusion
  20.4 0.0 copy-done.5
  20.4 0.3 convolution_convert_fusion.3
  20.7 0.0 copy-done.11
  20.7 0.0 copy-start.9
  20.7 0.1 fusion.50
  20.9 0.0 copy-done.6
  20.9 0.0 copy-start.7
  20.9 0.2 convolution_convert_fusion.2
  21.1 7.9 %all-gather = bf16[96,2048]{1,0:T(8,128)(2,1)S(1)} all-gather(bf16[24,2048]{1,0:T(8,128)(2,1)S(1)} %convolution_convert_fusion.2), channel_id=2, replica_groups=mesh['ep'=8,'tp'=4] {'tp'}, dimensions={0}, use_global_device_ids=true | all-gather | bytes 491520 | tf_op jit(solution)/shard_map/all_gather | solution.py:46
  29.1 0.1 fusion.30
  29.3 0.1 copy.40
  29.4 0.1 eq.55
  29.5 0.2 convert_reduce_fusion.2
  29.7 0.1 reduce_sum.98
  29.8 0.1 copy.45
  29.9 0.1 fusion.40
  30.0 0.3 convolution_convert_fusion.1
  30.3 0.8 %reshape.182 = bf16[8,7,2048]{2,1,0:T(8,128)(2,1)} reshape(bf16[56,2048]{1,0:T(8,128)(2,1)S(1)} %convolution_convert_fusion.1) | data formatting | bytes 458752 | tf_op jit(solution)/shard_map/reshape | solution.py:138
  31.1 5.8 %all-to-all-start = ((bf16[8,7,2048]{2,1,0:T(8,128)(2,1)}), bf16[8,7,2048]{2,1,0:T(8,128)(2,1)S(1)}, u32[]{:S(2)}, u32[]{:S(2)}) async-start(bf16[8,7,2048]{2,1,0:T(8,128)(2,1)} %reshape.182), calls=%async_computation | async-start | bytes 524288 | tf_op jit(solution)/shard_map/all_to_all | solution.py:139
  36.9 0.2 fusion.25
  37.1 0.0 copy-done.7
  37.2 2.0 %fusion.67 = f32[24,512]{1,0:T(8,128)S(1)} fusion(bf16[2048,512]{1,0:T(8,128)(2,1)} %param.38, bf16[24,2048]{1,0:T(8,128)(2,1)S(1)} %get-tuple-element.3, f32[2048]{0:T(1024)S(1)} %convert_element_type.101, f32[24]{0:T(128)S(1)} %add_rsqrt_fusion.3), kind=kOutput, calls=%fused_computation.112 | convolution fusion | flops 50528256 | bytes 2252896 | tf_op jit(solution)/shard_map/dot_general | solution.py:115
  39.2 7.1 %all-to-all-done = bf16[8,7,2048]{2,1,0:T(8,128)(2,1)S(1)} async-done(((bf16[8,7,2048]{2,1,0:T(8,128)(2,1)}), bf16[8,7,2048]{2,1,0:T(8,128)(2,1)S(1)}, u32[]{:S(2)}, u32[]{:S(2)}) %all-to-all-start) | async-done | bytes 229408 | tf_op jit(solution)/shard_map/all_to_all | solution.py:139
  46.3 0.1 reshape.183
  46.4 2.0 %fusion.7 = f32[56,512]{1,0:T(8,128)S(1)} fusion(bf16[56,2048]{1,0:T(8,128)(2,1)S(1)} %reshape.183, bf16[1,2048,512]{2,1,0:T(8,128)(2,1)} %param.41), kind=kOutput, calls=%fused_computation.13 | convolution fusion | flops 117440512 | bytes 2441216 | tf_op jit(solution)/shard_map/dot_general | solution.py:51
  48.5 2.5 %convolution_convert_fusion = bf16[56,2048]{1,0:T(8,128)(2,1)S(1)} fusion(bf16[1,512,2048]{2,1,0:T(8,128)(2,1)S(1)} %copy-done, bf16[56,2048]{1,0:T(8,128)(2,1)S(1)} %reshape.183, bf16[1,2048,512]{2,1,0:T(8,128)(2,1)} %param.42, f32[56,512]{1,0:T(8,128)S(1)} %fusion.7), kind=kOutput, calls=%fused_computation.3 | convolution fusion | flops 235167744 | bytes 4767744 | tf_op jit(solution)/shard_map/dot_general | solution.py:54
  50.9 0.8 %reshape.184 = bf16[8,7,2048]{2,1,0:T(8,128)(2,1)} reshape(bf16[56,2048]{1,0:T(8,128)(2,1)S(1)} %convolution_convert_fusion) | data formatting | bytes 458752 | tf_op jit(solution)/shard_map/reshape | solution.py:144
  51.7 3.6 %all-to-all-start.1 = ((bf16[8,7,2048]{2,1,0:T(8,128)(2,1)}), bf16[8,7,2048]{2,1,0:T(8,128)(2,1)S(1)}, u32[]{:S(2)}, u32[]{:S(2)}) async-start(bf16[8,7,2048]{2,1,0:T(8,128)(2,1)} %reshape.184), calls=%async_computation.1 | async-start | bytes 524288 | tf_op jit(solution)/shard_map/all_to_all | solution.py:143
  55.3 0.1 select_reduce_fusion
  55.4 3.0 %convolution_multiply_fusion = f32[24,2048]{1,0:T(8,128)S(1)} fusion(bf16[512,2048]{1,0:T(8,128)(2,1)} %param.40, bf16[2048,512]{1,0:T(8,128)(2,1)} %param.39, f32[24]{0:T(128)S(1)} %fusion.25, f32[24,512]{1,0:T(8,128)S(1)} %fusion.67, bf16[24,2048]{1,0:T(8,128)(2,1)S(1)} %get-tuple-element.3, f32[2048]{0:T(1024)S(1)} %convert_element_type.101, ...), kind=kOutput, calls=%fused_computation.7 | convolution fusion | flops 100982784 | bytes 4546752 | tf_op jit(solution)/shard_map/dot_general | solution.py:118
  58.4 5.9 %all-to-all-done.1 = bf16[8,7,2048]{2,1,0:T(8,128)(2,1)S(1)} async-done(((bf16[8,7,2048]{2,1,0:T(8,128)(2,1)}), bf16[8,7,2048]{2,1,0:T(8,128)(2,1)S(1)}, u32[]{:S(2)}, u32[]{:S(2)}) %all-to-all-start.1) | async-done | bytes 229408 | tf_op jit(solution)/shard_map/all_to_all | solution.py:143
  64.3 0.1 reshape.185
  64.4 0.2 fusion.61
  64.6 0.2 fusion.3
  64.7 6.1 %all-gather.1 = bf16[96,2048]{1,0:T(8,128)(2,1)S(1)} all-gather(bf16[24,2048]{1,0:T(8,128)(2,1)S(1)} %fusion.3), channel_id=3, replica_groups=mesh['ep'=8,'tp'=4] {'tp'}, dimensions={0}, use_global_device_ids=true | all-gather | bytes 491520 | tf_op jit(solution)/shard_map/all_gather | solution.py:46
  70.9 0.7 fusion.33
  (27 shorter events, 0.4 us)
Async XLA Ops:
  0.6 47.8 %copy-start = (bf16[1,512,2048]{2,1,0:T(8,128)(2,1)S(1)}, bf16[1,512,2048]{2,1,0:T(8,128)(2,1)}, u32[]{:S(2)}) copy-start(bf16[1,512,2048]{2,1,0:T(8,128)(2,1)} %param.43) | copy-start | bytes 6291460
  0.6 8.4 %copy-start.3 = (bf16[24,2048]{1,0:T(8,128)(2,1)S(1)}, bf16[24,2048]{1,0:T(8,128)(2,1)}, u32[]{:S(2)}) copy-start(bf16[24,2048]{1,0:T(8,128)(2,1)} %param.23) | copy-start | bytes 294916
  0.7 8.4 %copy-start.4 = (bf16[2048,256]{1,0:T(8,128)(2,1)S(1)}, bf16[2048,256]{1,0:T(8,128)(2,1)}, u32[]{:S(2)}) copy-start(bf16[2048,256]{1,0:T(8,128)(2,1)} %param.26) | copy-start | bytes 3145732
  9.4 5.3 %copy-start.1 = (f32[24,2,128,128]{3,2,1,0:T(8,128)S(1)}, f32[24,2,128,128]{3,2,1,0:T(8,128)}, u32[]{:S(2)}) copy-start(f32[24,2,128,128]{3,2,1,0:T(8,128)} %param.24) | copy-start | bytes 9437188
  15.8 1.7 %copy-start.2 = (f32[24,2,128,128]{3,2,1,0:T(8,128)}, f32[24,2,128,128]{3,2,1,0:T(8,128)S(1)}, u32[]{:S(2)}) copy-start(f32[24,2,128,128]{3,2,1,0:T(8,128)S(1)} %multiply_add_fusion) | copy-start | bytes 9437188
  15.8 4.6 %copy-start.5 = (bf16[2048,256]{1,0:T(8,128)(2,1)S(1)}, bf16[2048,256]{1,0:T(8,128)(2,1)}, u32[]{:S(2)}) copy-start(bf16[2048,256]{1,0:T(8,128)(2,1)} %param.29) | copy-start | bytes 3145732
  17.5 3.2 %copy-start.11 = (bf16[128]{0:T(256)(128)(2,1)S(1)}, bf16[128]{0:T(256)(128)(2,1)}, u32[]{:S(2)}) copy-start(bf16[128]{0:T(256)(128)(2,1)} %param.34) | copy-start | bytes 772
  17.5 3.4 %copy-start.6 = (bf16[256,2048]{1,0:T(8,128)(2,1)S(1)}, bf16[256,2048]{1,0:T(8,128)(2,1)}, u32[]{:S(2)}) copy-start(bf16[256,2048]{1,0:T(8,128)(2,1)} %param.35) | copy-start | bytes 3145732
  20.2 9.0 %copy-start.10 = (s32[24,6]{0,1:T(8,128)S(1)}, s32[24,6]{0,1:T(8,128)}, u32[]{:S(2)}) copy-start(s32[24,6]{0,1:T(8,128)} %param.44) | copy-start | bytes 1732
  20.2 9.7 %copy-start.8 = (bf16[2048]{0:T(1024)(128)(2,1)S(1)}, bf16[2048]{0:T(1024)(128)(2,1)}, u32[]{:S(2)}) copy-start(bf16[2048]{0:T(1024)(128)(2,1)} %param.36) | copy-start | bytes 12292
  20.7 16.2 %copy-start.9 = (bf16[2048]{0:T(1024)(128)(2,1)S(1)}, bf16[2048]{0:T(1024)(128)(2,1)}, u32[]{:S(2)}) copy-start(bf16[2048]{0:T(1024)(128)(2,1)} %param.37) | copy-start | bytes 12292
  20.9 16.3 %copy-start.7 = (f32[24,6]{0,1:T(8,128)S(1)}, f32[24,6]{0,1:T(8,128)}, u32[]{:S(2)}) copy-start(f32[24,6]{0,1:T(8,128)} %param.45) | copy-start | bytes 1732
  31.1 15.3 %all-to-all-start = ((bf16[8,7,2048]{2,1,0:T(8,128)(2,1)}), bf16[8,7,2048]{2,1,0:T(8,128)(2,1)S(1)}, u32[]{:S(2)}, u32[]{:S(2)}) async-start(bf16[8,7,2048]{2,1,0:T(8,128)(2,1)} %reshape.182), calls=%async_computation | async-start | bytes 524288 | tf_op jit(solution)/shard_map/all_to_all | solution.py:139
  51.7 12.6 %all-to-all-start.1 = ((bf16[8,7,2048]{2,1,0:T(8,128)(2,1)}), bf16[8,7,2048]{2,1,0:T(8,128)(2,1)S(1)}, u32[]{:S(2)}, u32[]{:S(2)}) async-start(bf16[8,7,2048]{2,1,0:T(8,128)(2,1)} %reshape.184), calls=%async_computation.1 | async-start | bytes 524288 | tf_op jit(solution)/shard_map/all_to_all | solution.py:143

commit v2 on v1

--- a/solution.py
+++ b/solution.py
@@ -27,13 +27,14 @@
     query_unit = unit_rows(jax.nn.silu(query_raw)) * head_size ** (-0.5)
     key_unit = unit_rows(jax.nn.silu(key_raw))
     value_act = jax.nn.silu(value_raw)
-    decayed = jnp.exp(log_decay)[:, :, None, None] * delta_state
-    predicted = jnp.einsum("shkv,shk->shv", decayed, key_unit, precision=lax.Precision.HIGHEST)
-    update = (beta_gate[:, :, None] * key_unit)[:, :, :, None] * (value_act - predicted)[
-        :, :, None, :
-    ]
-    new_state = decayed + update
-    readout = jnp.einsum("shkv,shk->shv", new_state, query_unit, precision=lax.Precision.HIGHEST)
+    decay = jnp.exp(log_decay)[:, :, None]
+    weighted_key = beta_gate[:, :, None] * key_unit
+    predicted = decay * jnp.sum(delta_state * key_unit[:, :, :, None], axis=2)
+    carried = decay * jnp.sum(delta_state * query_unit[:, :, :, None], axis=2)
+    error = value_act - predicted
+    overlap = jnp.sum(weighted_key * query_unit, axis=-1, keepdims=True)
+    new_state = decay[:, :, :, None] * delta_state + weighted_key[:, :, :, None] * error[:, :, None, :]
+    readout = carried + overlap * error
     return (new_state, readout)
 
 
@@ -100,7 +101,7 @@
     beta_all = jax.nn.sigmoid(jnp.dot(normed, beta_weight, preferred_element_type=jnp.float32))
     beta_gate = lax.dynamic_slice_in_dim(beta_all, head_start, head_local, 1)
     decay_input = jnp.dot(normed, decay_weight, preferred_element_type=jnp.float32) + decay_bias
-    decay_all = -decay_rate * jax.nn.softplus(decay_input)
+    decay_all = decay_rate * -jax.nn.softplus(decay_input)
     log_decay = lax.dynamic_slice_in_dim(decay_all, head_start, head_local, 1)
     new_state, readout = delta_update(
         delta_state, query_raw, key_raw, value_raw, beta_gate, log_decay
@@ -118,6 +119,8 @@
     dense_part = jnp.dot(dense_hidden, dense_down_weight, preferred_element_type=jnp.float32)
     expert_count = ep_count * tp_count
     capacity = max(2, (3 * seq_count * top_count + 2 * expert_count - 1) // (2 * expert_count))
+    if capacity > 4:
+        capacity = -(-capacity // 8) * 8
     flat_ids = route_ids.reshape(-1)
     assign_count = flat_ids.shape[0]
     earlier = jnp.arange(assign_count)[:, None] > jnp.arange(assign_count)[None, :]

time: 72.2 us -> 68.1 us (0.943)
  other arithmetic: 5.76 us -> 12.7 us
  matrix products: 24.4 us -> 19.4 us
  waiting for transfers between devices: 13 us -> 9.38 us
  local copies, waits for them, and re-layouts: 3.98 us -> 1.5 us
    dot_general x2 -> x0, matrix products: 7.71 us -> none  [the longest x1 4.94 us: delta_update(): jnp.einsum('shkv,shk->shv', decayed, key_unit, precision=lax.Precision.HI...]
    reduce_sum x0 -> x2, other arithmetic: none -> 4.06 us  [the longest x1 3.84 us: delta_update(): predicted = decay * jnp.sum(delta_state * key_unit[:, :, :, None], axis=2)]
    all_to_all x1, waiting for transfers between devices: 7.12 us -> 4.1 us  [shards(): lax.all_to_all(outgoing, 'ep', split_axis=0, concat_axis=0, tiled=True)]
    add x1, other arithmetic: 1.1 us -> 3.6 us  [delta_update(): decay[:, :, :, None] * delta_state]
    reshape x4 -> x0, local copies, waits for them, and re-layouts: 1.72 us -> none  [the longest x1 0.78 us: shards(): outgoing = outgoing.reshape(ep_count, capacity, model_width)]
    convert_element_type x3, other arithmetic: 0.85 us -> 2.2 us  [rms_scale(): return values * inverse * gain.astype(jnp.float32)]
    dot_general x4, matrix products: 3.74 us -> 4.96 us  [project(): product = jnp.dot(normed, weight, preferred_element_type=jnp.float32)]
    unnamed x26 -> x14, local copies, waits for them, and re-layouts: 1.7 us -> 0.81 us
  transfers between devices with their start and end apart: 2 -> 2, of which waited for: 2 -> 2; matrix products, arithmetic and copies ran while one was open for 8% -> 13% of each run, Pallas kernels for 0% -> 0%
where the time goes in v2:
time: 68.1 us; the launch traced here: 67.3 us
  matrix products  19.4 us (28%)
  blocking collectives  14.1 us (21%)
  other arithmetic  12.7 us (19%)
  starting transfers between devices  9.43 us (14%)
  waiting for transfers between devices  9.38 us (14%)
  local copies, waits for them, and re-layouts  1.5 us (2%)
  between operations  0.89 us (1%)
    all_gather x2, blocking collectives, tp_sum(): parts = lax.all_gather(part.astype(jnp.bfloat16), 'tp', axis=0, tiled=False)  14.1 us
    all_to_all x1, starting transfers between devices, shards(): lax.all_to_all(outgoing, 'ep', split_axis=0, concat_axis=0, tiled=True)  5.84 us
    all_to_all x1, waiting for transfers between devices, shards(): lax.all_to_all(result.reshape(arrived.shape), 'ep', split_axis=0, concat_...  5.28 us
    dot_general x4, matrix products, project(): product = jnp.dot(normed, weight, preferred_element_type=jnp.float32)  4.96 us
    all_to_all x1, waiting for transfers between devices, shards(): lax.all_to_all(outgoing, 'ep', split_axis=0, concat_axis=0, tiled=True)  4.1 us
    reduce_sum x1, other arithmetic, delta_update(): predicted = decay * jnp.sum(delta_state * key_unit[:, :, :, None], axis=2)  3.84 us
    add x1, other arithmetic, delta_update(): decay[:, :, :, None] * delta_state  3.6 us
    all_to_all x1, starting transfers between devices, shards(): lax.all_to_all(result.reshape(arrived.shape), 'ep', split_axis=0, concat_...  3.59 us
  transfers between devices with their start and end apart: 2, of which 2 were waited for; matrix products, arithmetic and copies ran while one was open for 13% of the time, Pallas kernels for 0%

profile of v2, /device:TPU:0, one launch (start us, length us, event | category | flops | bytes accessed | tf_op | source)
XLA Modules:
  0.0 67.3 jit_solution(359225959966421222)
XLA Ops:
  0.6 0.0 copy-start
  0.6 0.0 copy-start.1
  0.7 0.0 copy-start.2
  0.7 0.8 %convert_element_type.93 = f32[128]{0:T(128)S(1)} convert(bf16[128]{0:T(256)(128)(2,1)} %param.34) | non-fusion elementwise | flops 128 | bytes 768 | tf_op jit(solution)/shard_map/convert_element_type | solution.py:14
  1.5 1.1 %fusion.31 = f32[24]{0:T(128)S(1)} fusion(bf16[24,2048]{1,0:T(8,128)(2,1)} %param.23), kind=kLoop, calls=%fused_computation.48 | loop fusion | flops 147432 | bytes 98400 | tf_op jit(solution)/shard_map/reduce_sum | solution.py:13
  2.6 0.7 %convert_element_type.87 = f32[2048]{0:T(1024)S(1)} convert(bf16[2048]{0:T(1024)(128)(2,1)} %param.25) | non-fusion elementwise | flops 2048 | bytes 12288 | tf_op jit(solution)/shard_map/convert_element_type | solution.py:14
  3.3 0.7 %convert_element_type.103 = f32[2048]{0:T(1024)S(1)} convert(bf16[2048]{0:T(1024)(128)(2,1)} %param.36) | non-fusion elementwise | flops 2048 | bytes 12288 | tf_op jit(solution)/shard_map/convert_element_type | solution.py:14
  4.0 1.1 %fusion.18 = f32[24,8]{0,1:T(8,128)S(1)} fusion(bf16[2048,8]{0,1:T(8,128)(2,1)} %param.30, bf16[24,2048]{1,0:T(8,128)(2,1)} %param.23, f32[2048]{0:T(1024)S(1)} %convert_element_type.87, f32[24]{0:T(128)S(1)} %add_rsqrt_fusion.4), kind=kOutput, calls=%fused_computation.28 | convolution fusion | flops 983616 | bytes 140128 | tf_op jit(solution)/shard_map/dot_general | solution.py:101
  5.1 1.2 %fusion.75 = f32[24,8]{0,1:T(8,128)S(1)} fusion(bf16[2048,8]{0,1:T(8,128)(2,1)} %param.31, f32[8]{0:T(128)} %param.33, f32[8]{0:T(128)} %param.32, bf16[24,2048]{1,0:T(8,128)(2,1)} %param.23, f32[2048]{0:T(1024)S(1)} %convert_element_type.87, f32[24]{0:T(128)S(1)} %add_rsqrt_fusion.4), kind=kOutput, calls=%fused_computation.123 | convolution fusion | flops 984768 | bytes 140192 | tf_op jit(solution)/shard_map/dot_general | solution.py:103
  6.3 0.1 copy.40
  6.3 0.8 %copy.42 = s32[24,6]{1,0:T(8,128)S(1)} copy(s32[24,6]{0,1:T(8,128)} %param.44) | data formatting | bytes 1152 | tf_op args[21]
  7.1 0.1 eq.55
  7.2 0.2 convert_reduce_fusion.2
  7.4 0.1 reduce_sum.128
  7.5 0.1 copy.47
  7.6 0.1 fusion.45
  7.7 0.1 copy.41
  7.8 1.6 %convolution_convert_fusion.6 = bf16[24,256]{1,0:T(8,128)(2,1)S(1)} fusion(bf16[2048,256]{1,0:T(8,128)(2,1)} %param.26, bf16[24,2048]{1,0:T(8,128)(2,1)} %param.23, f32[2048]{0:T(1024)S(1)} %convert_element_type.87, f32[24]{0:T(128)S(1)} %add_rsqrt_fusion.4), kind=kOutput, calls=%fused_computation.24 | convolution fusion | flops 25368576 | bytes 1167456 | tf_op jit(solution)/shard_map/dot_general | solution.py:93
  9.4 1.6 %convolution_convert_fusion.5 = bf16[24,256]{1,0:T(8,128)(2,1)S(1)} fusion(bf16[2048,256]{1,0:T(8,128)(2,1)} %param.27, bf16[24,2048]{1,0:T(8,128)(2,1)} %param.23, f32[2048]{0:T(1024)S(1)} %convert_element_type.87, f32[24]{0:T(128)S(1)} %add_rsqrt_fusion.4), kind=kOutput, calls=%fused_computation.23 | convolution fusion | flops 25368576 | bytes 1167456 | tf_op jit(solution)/shard_map/dot_general | solution.py:93
  11.0 0.0 copy-done.1
  11.0 0.0 copy-done.2
  11.0 0.3 convolution_convert_fusion.4
  11.3 1.5 %convolution_convert_fusion.3 = bf16[24,256]{1,0:T(8,128)(2,1)S(1)} fusion(bf16[2048,256]{1,0:T(8,128)(2,1)} %param.29, bf16[24,2048]{1,0:T(8,128)(2,1)S(1)} %copy-done.1, f32[2048]{0:T(1024)S(1)} %convert_element_type.87, f32[24]{0:T(128)S(1)} %add_rsqrt_fusion.4), kind=kOutput, calls=%fused_computation.21 | convolution fusion | flops 25368576 | bytes 1167456 | tf_op jit(solution)/shard_map/dot_general | solution.py:93
  12.9 0.0 copy-start.3
  12.9 0.1 multiply_reduce_fusion.4
  13.1 0.2 multiply_reduce_fusion.3
  13.3 3.8 %multiply_reduce_fusion = (f32[24,2,128]{2,1,0:T(2,128)S(1)}, f32[24,2,128]{2,1,0:T(2,128)S(1)}) fusion(f32[24,2,128,128]{3,2,1,0:T(8,128)} %param.24, f32[24,2,128]{2,1,0:T(2,128)S(1)} %get-tuple-element.13, f32[24,2,128]{2,1,0:T(2,128)S(1)} %get-tuple-element.12), kind=kLoop, calls=%fused_computation.1 | loop fusion | flops 3133440 | bytes 3244032 | tf_op jit(solution)/shard_map/reduce_sum | solution.py:32
  17.1 0.0 copy-start.5
  17.1 0.2 multiply_reduce_fusion.2
  17.4 0.1 mul.310
  17.5 0.1 mul.321
  17.5 0.0 copy-done.3
  17.6 0.3 convolution_convert_fusion.2
  17.8 7.9 %all-gather = bf16[96,2048]{1,0:T(8,128)(2,1)S(1)} all-gather(bf16[24,2048]{1,0:T(8,128)(2,1)S(1)} %convolution_convert_fusion.2), channel_id=2, replica_groups=mesh['ep'=8,'tp'=4] {'tp'}, dimensions={0}, use_global_device_ids=true | all-gather | bytes 491520 | tf_op jit(solution)/shard_map/all_gather | solution.py:47
  25.8 0.0 copy-start.4
  25.8 0.1 fusion.35
  26.0 1.0 %fusion = bf16[8,8,2048]{2,1,0:T(8,128)(2,1)} fusion(pred[64,24]{0,1:T(8,128)(4,1)S(1)} %fusion.45, bf16[24,2048]{1,0:T(8,128)(2,1)S(1)} %get-tuple-element.5, f32[2048]{0:T(1024)S(1)} %convert_element_type.103, f32[24]{0:T(128)S(1)} %add_rsqrt_fusion.3), kind=kOutput, calls=%fused_computation.5 | convolution fusion | flops 6619136 | bytes 370272 | tf_op jit(solution)/shard_map/dot_general | solution.py:138
  27.0 5.8 %all-to-all-start = ((bf16[8,8,2048]{2,1,0:T(8,128)(2,1)}), bf16[8,8,2048]{2,1,0:T(8,128)(2,1)S(1)}, u32[]{:S(2)}, u32[]{:S(2)}) async-start(bf16[8,8,2048]{2,1,0:T(8,128)(2,1)} %fusion), calls=%async_computation | async-start | bytes 524288 | tf_op jit(solution)/shard_map/all_to_all | solution.py:142
  32.8 0.0 copy-done.5
  32.8 0.2 fusion.22
  33.1 2.0 %fusion.81 = f32[24,512]{1,0:T(8,128)S(1)} fusion(bf16[2048,512]{1,0:T(8,128)(2,1)} %param.38, bf16[24,2048]{1,0:T(8,128)(2,1)S(1)} %get-tuple-element.5, f32[2048]{0:T(1024)S(1)} %convert_element_type.103, f32[24]{0:T(128)S(1)} %add_rsqrt_fusion.3), kind=kOutput, calls=%fused_computation.133 | convolution fusion | flops 50528256 | bytes 2252896 | tf_op jit(solution)/shard_map/dot_general | solution.py:116
  35.1 0.0 copy-done.4
  35.1 3.0 %convolution_multiply_fusion = f32[24,2048]{1,0:T(8,128)S(1)} fusion(bf16[512,2048]{1,0:T(8,128)(2,1)} %param.40, bf16[2048,512]{1,0:T(8,128)(2,1)} %param.39, f32[24]{0:T(128)S(1)} %fusion.22, f32[24,512]{1,0:T(8,128)S(1)} %fusion.81, bf16[24,2048]{1,0:T(8,128)(2,1)S(1)} %get-tuple-element.5, f32[2048]{0:T(1024)S(1)} %convert_element_type.103, ...), kind=kOutput, calls=%fused_computation.9 | convolution fusion | flops 100982784 | bytes 4546752 | tf_op jit(solution)/shard_map/dot_general | solution.py:119
  38.1 4.1 %all-to-all-done = bf16[8,8,2048]{2,1,0:T(8,128)(2,1)S(1)} async-done(((bf16[8,8,2048]{2,1,0:T(8,128)(2,1)}), bf16[8,8,2048]{2,1,0:T(8,128)(2,1)S(1)}, u32[]{:S(2)}, u32[]{:S(2)}) %all-to-all-start) | async-done | bytes 262176 | tf_op jit(solution)/shard_map/all_to_all | solution.py:142
  42.2 2.1 %fusion.7 = f32[64,512]{1,0:T(8,128)S(1)} fusion(bf16[1,2048,512]{2,1,0:T(8,128)(2,1)} %param.41, bf16[8,8,2048]{2,1,0:T(8,128)(2,1)S(1)} %all-to-all-done), kind=kOutput, calls=%fused_computation.15 | convolution fusion | flops 134217728 | bytes 2490368 | tf_op jit(solution)/shard_map/dot_general | solution.py:52
  44.3 0.0 copy-done
  44.3 3.2 %fusion.1 = bf16[8,8,2048]{2,1,0:T(8,128)(2,1)} fusion(bf16[1,512,2048]{2,1,0:T(8,128)(2,1)S(1)} %copy-done, bf16[1,2048,512]{2,1,0:T(8,128)(2,1)} %param.42, bf16[8,8,2048]{2,1,0:T(8,128)(2,1)S(1)} %all-to-all-done, f32[64,512]{1,0:T(8,128)S(1)} %fusion.7), kind=kOutput, calls=%fused_computation.6 | convolution fusion | flops 268763136 | bytes 4849664 | tf_op jit(solution)/shard_map/dot_general | solution.py:55
  47.5 3.6 %all-to-all-start.1 = ((bf16[8,8,2048]{2,1,0:T(8,128)(2,1)}), bf16[8,8,2048]{2,1,0:T(8,128)(2,1)S(1)}, u32[]{:S(2)}, u32[]{:S(2)}) async-start(bf16[8,8,2048]{2,1,0:T(8,128)(2,1)} %fusion.1), calls=%async_computation.1 | async-start | bytes 524288 | tf_op jit(solution)/shard_map/all_to_all | solution.py:146
  51.1 0.1 select_reduce_fusion
  51.2 3.6 %multiply_add_fusion = f32[24,2,128,128]{3,2,1,0:T(8,128)} fusion(f32[24,2,128,128]{3,2,1,0:T(8,128)} %param.24, f32[24,2,128]{2,1,0:T(2,128)S(1)} %get-tuple-element.7, f32[24,2,128]{2,1,0:T(2,128)S(1)} %get-tuple-element.11, f32[24,2]{1,0:T(8,128)S(1)} %copy.40), kind=kLoop, calls=%fused_computation | loop fusion | flops 2359296 | bytes 6340800 | tf_op jit(solution)/shard_map/add | solution.py:36
  54.8 5.3 %all-to-all-done.1 = bf16[8,8,2048]{2,1,0:T(8,128)(2,1)S(1)} async-done(((bf16[8,8,2048]{2,1,0:T(8,128)(2,1)}), bf16[8,8,2048]{2,1,0:T(8,128)(2,1)S(1)}, u32[]{:S(2)}, u32[]{:S(2)}) %all-to-all-start.1) | async-done | bytes 262176 | tf_op jit(solution)/shard_map/all_to_all | solution.py:146
  60.1 0.2 fusion.26
  60.3 0.2 fusion.3
  60.4 6.1 %all-gather.1 = bf16[96,2048]{1,0:T(8,128)(2,1)S(1)} all-gather(bf16[24,2048]{1,0:T(8,128)(2,1)S(1)} %fusion.3), channel_id=3, replica_groups=mesh['ep'=8,'tp'=4] {'tp'}, dimensions={0}, use_global_device_ids=true | all-gather | bytes 491520 | tf_op jit(solution)/shard_map/all_gather | solution.py:47
  66.6 0.7 fusion.38
  (16 shorter events, 0.3 us)
Async XLA Ops:
  0.6 43.7 %copy-start = (bf16[1,512,2048]{2,1,0:T(8,128)(2,1)S(1)}, bf16[1,512,2048]{2,1,0:T(8,128)(2,1)}, u32[]{:S(2)}) copy-start(bf16[1,512,2048]{2,1,0:T(8,128)(2,1)} %param.43) | copy-start | bytes 6291460
  0.6 10.4 %copy-start.1 = (bf16[24,2048]{1,0:T(8,128)(2,1)S(1)}, bf16[24,2048]{1,0:T(8,128)(2,1)}, u32[]{:S(2)}) copy-start(bf16[24,2048]{1,0:T(8,128)(2,1)} %param.23) | copy-start | bytes 294916
  0.7 10.4 %copy-start.2 = (bf16[2048,256]{1,0:T(8,128)(2,1)S(1)}, bf16[2048,256]{1,0:T(8,128)(2,1)}, u32[]{:S(2)}) copy-start(bf16[2048,256]{1,0:T(8,128)(2,1)} %param.28) | copy-start | bytes 3145732
  12.9 4.7 %copy-start.3 = (bf16[256,2048]{1,0:T(8,128)(2,1)S(1)}, bf16[256,2048]{1,0:T(8,128)(2,1)}, u32[]{:S(2)}) copy-start(bf16[256,2048]{1,0:T(8,128)(2,1)} %param.35) | copy-start | bytes 3145732
  17.1 15.7 %copy-start.5 = (bf16[2048]{0:T(1024)(128)(2,1)S(1)}, bf16[2048]{0:T(1024)(128)(2,1)}, u32[]{:S(2)}) copy-start(bf16[2048]{0:T(1024)(128)(2,1)} %param.37) | copy-start | bytes 12292
  25.8 9.3 %copy-start.4 = (f32[24,6]{0,1:T(8,128)S(1)}, f32[24,6]{0,1:T(8,128)}, u32[]{:S(2)}) copy-start(f32[24,6]{0,1:T(8,128)} %param.45) | copy-start | bytes 1732
  27.0 15.3 %all-to-all-start = ((bf16[8,8,2048]{2,1,0:T(8,128)(2,1)}), bf16[8,8,2048]{2,1,0:T(8,128)(2,1)S(1)}, u32[]{:S(2)}, u32[]{:S(2)}) async-start(bf16[8,8,2048]{2,1,0:T(8,128)(2,1)} %fusion), calls=%async_computation | async-start | bytes 524288 | tf_op jit(solution)/shard_map/all_to_all | solution.py:142
  47.5 12.6 %all-to-all-start.1 = ((bf16[8,8,2048]{2,1,0:T(8,128)(2,1)}), bf16[8,8,2048]{2,1,0:T(8,128)(2,1)S(1)}, u32[]{:S(2)}, u32[]{:S(2)}) async-start(bf16[8,8,2048]{2,1,0:T(8,128)(2,1)} %fusion.1), calls=%async_computation.1 | async-start | bytes 524288 | tf_op jit(solution)/shard_map/all_to_all | solution.py:146

commit v3 on v2

--- a/solution.py
+++ b/solution.py
@@ -87,7 +87,7 @@
     ep_count = lax.axis_size("ep")
     tp_count = lax.axis_size("tp")
     tp_index = lax.axis_index("tp")
-    normed = rms_scale(tokens, first_gain).astype(jnp.bfloat16)
+    normed = lax.optimization_barrier(rms_scale(tokens, first_gain).astype(jnp.bfloat16))
 
     def project(weight):
         product = jnp.dot(normed, weight, preferred_element_type=jnp.float32)
@@ -109,7 +109,7 @@
     gated = gated_heads(readout, outgate_raw, head_gain)
     mix_part = jnp.dot(gated, out_weight, preferred_element_type=jnp.float32)
     residual = (tokens.astype(jnp.float32) + tp_sum(mix_part)).astype(jnp.bfloat16)
-    normed_mid = rms_scale(residual, second_gain).astype(jnp.bfloat16)
+    normed_mid = lax.optimization_barrier(rms_scale(residual, second_gain).astype(jnp.bfloat16))
     blend_gate = jax.nn.sigmoid(
         jnp.dot(normed_mid, blend_weight, preferred_element_type=jnp.float32)
     )

time: 68.1 us -> 67.4 us (0.990)
  matrix products: 19.4 us -> 17.3 us
  other arithmetic: 12.7 us -> 13.7 us
    dot_general x4, matrix products: 4.96 us -> 3.56 us  [project(): product = jnp.dot(normed, weight, preferred_element_type=jnp.float32)]
    convert_element_type x0 -> x2, other arithmetic: none -> 1.08 us  [the longest x1 0.98 us: shards(): rms_scale(tokens, first_gain).astype(jnp.bfloat16)]
where the time goes in v3:
time: 67.4 us; the launch traced here: 66.5 us
  matrix products  17.3 us (26%)
  blocking collectives  14.1 us (21%)
  other arithmetic  13.7 us (20%)
  waiting for transfers between devices  9.55 us (14%)
  starting transfers between devices  9.41 us (14%)
  local copies, waits for them, and re-layouts  1.5 us (2%)
  between operations  0.9 us (1%)
    all_gather x2, blocking collectives, tp_sum(): parts = lax.all_gather(part.astype(jnp.bfloat16), 'tp', axis=0, tiled=False)  14.1 us
    all_to_all x1, starting transfers between devices, shards(): lax.all_to_all(outgoing, 'ep', split_axis=0, concat_axis=0, tiled=True)  5.83 us
    all_to_all x1, waiting for transfers between devices, shards(): lax.all_to_all(result.reshape(arrived.shape), 'ep', split_axis=0, concat_...  5.29 us
    all_to_all x1, waiting for transfers between devices, shards(): lax.all_to_all(outgoing, 'ep', split_axis=0, concat_axis=0, tiled=True)  4.26 us
    reduce_sum x1, other arithmetic, delta_update(): predicted = decay * jnp.sum(delta_state * key_unit[:, :, :, None], axis=2)  3.83 us
    add x1, other arithmetic, delta_update(): decay[:, :, :, None] * delta_state  3.6 us
    all_to_all x1, starting transfers between devices, shards(): lax.all_to_all(result.reshape(arrived.shape), 'ep', split_axis=0, concat_...  3.59 us
    dot_general x4, matrix products, project(): product = jnp.dot(normed, weight, preferred_element_type=jnp.float32)  3.56 us
  transfers between devices with their start and end apart: 2, of which 2 were waited for; matrix products, arithmetic and copies ran while one was open for 13% of the time, Pallas kernels for 0%

profile of v3, /device:TPU:0, one launch (start us, length us, event | category | flops | bytes accessed | tf_op | source)
XLA Modules:
  0.0 66.5 jit_solution(6095087277204956211)
XLA Ops:
  0.6 0.0 copy-start
  0.6 0.0 copy-start.1
  0.7 0.8 %convert_element_type.93 = f32[128]{0:T(128)S(1)} convert(bf16[128]{0:T(256)(128)(2,1)} %param.34) | non-fusion elementwise | flops 128 | bytes 768 | tf_op jit(solution)/shard_map/convert_element_type | solution.py:14
  1.5 1.1 %fusion.31 = f32[24]{0:T(128)S(1)} fusion(bf16[24,2048]{1,0:T(8,128)(2,1)} %param.23), kind=kLoop, calls=%fused_computation.48 | loop fusion | flops 147432 | bytes 98400 | tf_op jit(solution)/shard_map/reduce_sum | solution.py:13
  2.6 0.7 %convert_element_type.87 = f32[2048]{0:T(1024)S(1)} convert(bf16[2048]{0:T(1024)(128)(2,1)} %param.25) | non-fusion elementwise | flops 2048 | bytes 12288 | tf_op jit(solution)/shard_map/convert_element_type | solution.py:14
  3.3 0.7 %convert_element_type.103 = f32[2048]{0:T(1024)S(1)} convert(bf16[2048]{0:T(1024)(128)(2,1)} %param.36) | non-fusion elementwise | flops 2048 | bytes 12288 | tf_op jit(solution)/shard_map/convert_element_type | solution.py:14
  3.9 0.8 %copy.42 = s32[24,6]{1,0:T(8,128)S(1)} copy(s32[24,6]{0,1:T(8,128)} %param.44) | data formatting | bytes 1152 | tf_op args[21]
  4.7 0.1 eq.55
  4.8 0.2 convert_reduce_fusion.2
  5.0 0.1 reduce_sum.128
  5.1 0.1 copy.47
  5.2 0.1 fusion.45
  5.3 1.0 %fusion.33 = bf16[24,2048]{1,0:T(8,128)(2,1)S(1)} fusion(bf16[24,2048]{1,0:T(8,128)(2,1)} %param.23, f32[2048]{0:T(1024)S(1)} %convert_element_type.87, f32[24]{0:T(128)S(1)} %add_rsqrt_fusion.4), kind=kLoop, calls=%fused_computation.50 | loop fusion | flops 196608 | bytes 204896 | tf_op jit(solution)/shard_map/convert_element_type | solution.py:90
  6.3 0.9 %fusion.18 = f32[24,8]{0,1:T(8,128)S(1)} fusion(bf16[24,2048]{1,0:T(8,128)(2,1)S(1)} %fusion.33, bf16[2048,8]{0,1:T(8,128)(2,1)} %param.30), kind=kOutput, calls=%fused_computation.28 | convolution fusion | flops 787008 | bytes 131840 | tf_op jit(solution)/shard_map/dot_general | solution.py:101
  7.2 0.9 %fusion.75 = f32[24,8]{0,1:T(8,128)S(1)} fusion(bf16[24,2048]{1,0:T(8,128)(2,1)S(1)} %fusion.33, bf16[2048,8]{0,1:T(8,128)(2,1)} %param.31, f32[8]{0:T(128)} %param.33, f32[8]{0:T(128)} %param.32), kind=kOutput, calls=%fused_computation.123 | convolution fusion | flops 788160 | bytes 131904 | tf_op jit(solution)/shard_map/dot_general | solution.py:103
  8.2 0.1 copy.40
  8.3 0.1 copy.41
  8.4 0.0 copy-start.2
  8.4 1.6 %convolution_convert_fusion.3 = bf16[24,256]{1,0:T(8,128)(2,1)S(1)} fusion(bf16[24,2048]{1,0:T(8,128)(2,1)S(1)} %fusion.33, bf16[2048,256]{1,0:T(8,128)(2,1)} %param.29), kind=kOutput, calls=%fused_computation.21 | convolution fusion | flops 25171968 | bytes 1159168 | tf_op jit(solution)/shard_map/dot_general | solution.py:93
  9.9 1.5 %convolution_convert_fusion.4 = bf16[24,256]{1,0:T(8,128)(2,1)S(1)} fusion(bf16[24,2048]{1,0:T(8,128)(2,1)S(1)} %fusion.33, bf16[2048,256]{1,0:T(8,128)(2,1)} %param.28), kind=kOutput, calls=%fused_computation.22 | convolution fusion | flops 25171968 | bytes 1159168 | tf_op jit(solution)/shard_map/dot_general | solution.py:93
  11.4 0.0 copy-done.1
  11.4 0.3 convolution_convert_fusion.5
  11.7 0.0 copy-done.2
  11.7 0.3 convolution_convert_fusion.6
  11.9 0.0 copy-start.3
  12.0 0.1 multiply_reduce_fusion.4
  12.2 0.2 multiply_reduce_fusion.3
  12.4 3.8 %multiply_reduce_fusion = (f32[24,2,128]{2,1,0:T(2,128)S(1)}, f32[24,2,128]{2,1,0:T(2,128)S(1)}) fusion(f32[24,2,128,128]{3,2,1,0:T(8,128)} %param.24, f32[24,2,128]{2,1,0:T(2,128)S(1)} %get-tuple-element.13, f32[24,2,128]{2,1,0:T(2,128)S(1)} %get-tuple-element.12), kind=kLoop, calls=%fused_computation.1 | loop fusion | flops 3133440 | bytes 3244032 | tf_op jit(solution)/shard_map/reduce_sum | solution.py:32
  16.3 0.0 copy-start.4
  16.3 0.0 copy-start.6
  16.3 0.2 multiply_reduce_fusion.2
  16.5 0.1 mul.310
  16.6 0.1 mul.321
  16.7 0.0 copy-done.3
  16.7 0.3 convolution_convert_fusion.2
  16.9 7.9 %all-gather = bf16[96,2048]{1,0:T(8,128)(2,1)S(1)} all-gather(bf16[24,2048]{1,0:T(8,128)(2,1)S(1)} %convolution_convert_fusion.2), channel_id=2, replica_groups=mesh['ep'=8,'tp'=4] {'tp'}, dimensions={0}, use_global_device_ids=true | all-gather | bytes 491520 | tf_op jit(solution)/shard_map/all_gather | solution.py:47
  24.9 0.0 copy-start.5
  24.9 0.0 copy-done.4
  25.0 0.1 fusion.35
  25.1 0.1 fusion.37
  25.2 1.0 %fusion = bf16[8,8,2048]{2,1,0:T(8,128)(2,1)} fusion(pred[64,24]{0,1:T(8,128)(4,1)S(1)} %fusion.45, bf16[24,2048]{1,0:T(8,128)(2,1)S(1)} %fusion.37), kind=kOutput, calls=%fused_computation.5 | convolution fusion | flops 6422528 | bytes 361984 | tf_op jit(solution)/shard_map/dot_general | solution.py:138
  26.2 5.8 %all-to-all-start = ((bf16[8,8,2048]{2,1,0:T(8,128)(2,1)}), bf16[8,8,2048]{2,1,0:T(8,128)(2,1)S(1)}, u32[]{:S(2)}, u32[]{:S(2)}) async-start(bf16[8,8,2048]{2,1,0:T(8,128)(2,1)} %fusion), calls=%async_computation | async-start | bytes 524288 | tf_op jit(solution)/shard_map/all_to_all | solution.py:142
  32.0 0.0 copy-done.6
  32.0 0.1 fusion.22
  32.2 2.0 %fusion.81 = f32[24,512]{1,0:T(8,128)S(1)} fusion(bf16[24,2048]{1,0:T(8,128)(2,1)S(1)} %fusion.37, bf16[2048,512]{1,0:T(8,128)(2,1)} %param.38), kind=kOutput, calls=%fused_computation.133 | convolution fusion | flops 50331648 | bytes 2244608 | tf_op jit(solution)/shard_map/dot_general | solution.py:116
  34.2 0.0 copy-done.5
  34.2 3.0 %convolution_multiply_fusion = f32[24,2048]{1,0:T(8,128)S(1)} fusion(bf16[512,2048]{1,0:T(8,128)(2,1)} %param.40, bf16[24,2048]{1,0:T(8,128)(2,1)S(1)} %fusion.37, bf16[2048,512]{1,0:T(8,128)(2,1)} %param.39, f32[24]{0:T(128)S(1)} %fusion.22, f32[24,512]{1,0:T(8,128)S(1)} %fusion.81), kind=kOutput, calls=%fused_computation.9 | convolution fusion | flops 100786176 | bytes 4538464 | tf_op jit(solution)/shard_map/dot_general | solution.py:119
  37.2 4.3 %all-to-all-done = bf16[8,8,2048]{2,1,0:T(8,128)(2,1)S(1)} async-done(((bf16[8,8,2048]{2,1,0:T(8,128)(2,1)}), bf16[8,8,2048]{2,1,0:T(8,128)(2,1)S(1)}, u32[]{:S(2)}, u32[]{:S(2)}) %all-to-all-start) | async-done | bytes 262176 | tf_op jit(solution)/shard_map/all_to_all | solution.py:142
  41.5 2.1 %fusion.7 = f32[64,512]{1,0:T(8,128)S(1)} fusion(bf16[1,2048,512]{2,1,0:T(8,128)(2,1)} %param.41, bf16[8,8,2048]{2,1,0:T(8,128)(2,1)S(1)} %all-to-all-done), kind=kOutput, calls=%fused_computation.15 | convolution fusion | flops 134217728 | bytes 2490368 | tf_op jit(solution)/shard_map/dot_general | solution.py:52
  43.5 0.0 copy-done
  43.5 3.2 %fusion.1 = bf16[8,8,2048]{2,1,0:T(8,128)(2,1)} fusion(bf16[1,512,2048]{2,1,0:T(8,128)(2,1)S(1)} %copy-done, bf16[1,2048,512]{2,1,0:T(8,128)(2,1)} %param.42, bf16[8,8,2048]{2,1,0:T(8,128)(2,1)S(1)} %all-to-all-done, f32[64,512]{1,0:T(8,128)S(1)} %fusion.7), kind=kOutput, calls=%fused_computation.6 | convolution fusion | flops 268763136 | bytes 4849664 | tf_op jit(solution)/shard_map/dot_general | solution.py:55
  46.7 3.6 %all-to-all-start.1 = ((bf16[8,8,2048]{2,1,0:T(8,128)(2,1)}), bf16[8,8,2048]{2,1,0:T(8,128)(2,1)S(1)}, u32[]{:S(2)}, u32[]{:S(2)}) async-start(bf16[8,8,2048]{2,1,0:T(8,128)(2,1)} %fusion.1), calls=%async_computation.1 | async-start | bytes 524288 | tf_op jit(solution)/shard_map/all_to_all | solution.py:146
  50.3 0.1 select_reduce_fusion
  50.4 3.6 %multiply_add_fusion = f32[24,2,128,128]{3,2,1,0:T(8,128)} fusion(f32[24,2,128,128]{3,2,1,0:T(8,128)} %param.24, f32[24,2,128]{2,1,0:T(2,128)S(1)} %get-tuple-element.7, f32[24,2,128]{2,1,0:T(2,128)S(1)} %get-tuple-element.11, f32[24,2]{1,0:T(8,128)S(1)} %copy.40), kind=kLoop, calls=%fused_computation | loop fusion | flops 2359296 | bytes 6340800 | tf_op jit(solution)/shard_map/add | solution.py:36
  54.0 5.3 %all-to-all-done.1 = bf16[8,8,2048]{2,1,0:T(8,128)(2,1)S(1)} async-done(((bf16[8,8,2048]{2,1,0:T(8,128)(2,1)}), bf16[8,8,2048]{2,1,0:T(8,128)(2,1)S(1)}, u32[]{:S(2)}, u32[]{:S(2)}) %all-to-all-start.1) | async-done | bytes 262176 | tf_op jit(solution)/shard_map/all_to_all | solution.py:146
  59.3 0.2 fusion.26
  59.5 0.2 fusion.3
  59.7 6.1 %all-gather.1 = bf16[96,2048]{1,0:T(8,128)(2,1)S(1)} all-gather(bf16[24,2048]{1,0:T(8,128)(2,1)S(1)} %fusion.3), channel_id=3, replica_groups=mesh['ep'=8,'tp'=4] {'tp'}, dimensions={0}, use_global_device_ids=true | all-gather | bytes 491520 | tf_op jit(solution)/shard_map/all_gather | solution.py:47
  65.9 0.7 %fusion.38 = bf16[24,2048]{1,0:T(8,128)(2,1)} fusion(f32[24,2048]{1,0:T(8,128)S(1)} %convert_reduce_fusion, bf16[24,2048]{1,0:T(8,128)(2,1)S(1)} %get-tuple-element.5), kind=kLoop, calls=%fused_computation.55 | loop fusion | flops 147456 | bytes 393216 | tf_op jit(solution)/shard_map/convert_element_type | solution.py:163
  (16 shorter events, 0.3 us)
Async XLA Ops:
  0.6 42.9 %copy-start = (bf16[1,512,2048]{2,1,0:T(8,128)(2,1)S(1)}, bf16[1,512,2048]{2,1,0:T(8,128)(2,1)}, u32[]{:S(2)}) copy-start(bf16[1,512,2048]{2,1,0:T(8,128)(2,1)} %param.43) | copy-start | bytes 6291460
  0.6 10.8 %copy-start.1 = (bf16[2048,256]{1,0:T(8,128)(2,1)S(1)}, bf16[2048,256]{1,0:T(8,128)(2,1)}, u32[]{:S(2)}) copy-start(bf16[2048,256]{1,0:T(8,128)(2,1)} %param.27) | copy-start | bytes 3145732
  8.4 3.3 %copy-start.2 = (bf16[2048,256]{1,0:T(8,128)(2,1)S(1)}, bf16[2048,256]{1,0:T(8,128)(2,1)}, u32[]{:S(2)}) copy-start(bf16[2048,256]{1,0:T(8,128)(2,1)} %param.26) | copy-start | bytes 3145732
  11.9 4.7 %copy-start.3 = (bf16[256,2048]{1,0:T(8,128)(2,1)S(1)}, bf16[256,2048]{1,0:T(8,128)(2,1)}, u32[]{:S(2)}) copy-start(bf16[256,2048]{1,0:T(8,128)(2,1)} %param.35) | copy-start | bytes 3145732
  16.3 8.7 %copy-start.4 = (bf16[24,2048]{1,0:T(8,128)(2,1)S(1)}, bf16[24,2048]{1,0:T(8,128)(2,1)}, u32[]{:S(2)}) copy-start(bf16[24,2048]{1,0:T(8,128)(2,1)} %param.23) | copy-start | bytes 294916
  16.3 15.7 %copy-start.6 = (bf16[2048]{0:T(1024)(128)(2,1)S(1)}, bf16[2048]{0:T(1024)(128)(2,1)}, u32[]{:S(2)}) copy-start(bf16[2048]{0:T(1024)(128)(2,1)} %param.37) | copy-start | bytes 12292
  24.9 9.3 %copy-start.5 = (f32[24,6]{0,1:T(8,128)S(1)}, f32[24,6]{0,1:T(8,128)}, u32[]{:S(2)}) copy-start(f32[24,6]{0,1:T(8,128)} %param.45) | copy-start | bytes 1732
  26.2 15.3 %all-to-all-start = ((bf16[8,8,2048]{2,1,0:T(8,128)(2,1)}), bf16[8,8,2048]{2,1,0:T(8,128)(2,1)S(1)}, u32[]{:S(2)}, u32[]{:S(2)}) async-start(bf16[8,8,2048]{2,1,0:T(8,128)(2,1)} %fusion), calls=%async_computation | async-start | bytes 524288 | tf_op jit(solution)/shard_map/all_to_all | solution.py:142
  46.7 12.6 %all-to-all-start.1 = ((bf16[8,8,2048]{2,1,0:T(8,128)(2,1)}), bf16[8,8,2048]{2,1,0:T(8,128)(2,1)S(1)}, u32[]{:S(2)}, u32[]{:S(2)}) async-start(bf16[8,8,2048]{2,1,0:T(8,128)(2,1)} %fusion.1), calls=%async_computation.1 | async-start | bytes 524288 | tf_op jit(solution)/shard_map/all_to_all | solution.py:146
